TPU v7x, 256 devices: a whole 4x4x8 slice. The times are simulated.
256 devices in a mesh: sp: 32 (over z, y), tp: 8 (over x, core).
Axes of the slice: x: 4, y: 4, z: 8, core: 2. Of those that a mesh axis runs over, the one named last changes fastest.
Arguments:
- latent: bfloat16 [16384, 4096], P(('sp', 'tp')), may hold values from -3 to 3
- context: bfloat16 [1024, 4096], P('sp'), may hold values from -6 to 6
- cond: float32 [4096], replicated, may hold values from -6 to 6
- ctx_cond: float32 [4096], replicated, may hold values from -6 to 6
- w_shift: bfloat16 [4096, 4096], P('sp', 'tp'), may hold values from -0.1875 to 0.1875
- w_scale: bfloat16 [4096, 4096], P('sp', 'tp'), may hold values from -0.09375 to 0.15478516
- w_gate: bfloat16 [4096, 4096], P('sp', 'tp'), may hold values from -0.1875 to 0.1875
- w_query: bfloat16 [4096, 2048], P(None, 'tp'), may hold values from -0.09375 to 0.09375
- key_weight: bfloat16 [4096, 1024], P(None, 'tp'), may hold values from -0.09375 to 0.09375
- value_weight: bfloat16 [4096, 1024], P(None, 'tp'), may hold values from -0.09375 to 0.09375
- w_out: bfloat16 [2048, 4096], P('tp'), may hold values from -0.125 to 0.125
- sink: float32 [16], replicated, may hold values from 4 to 8
Outputs:
- mixed: bfloat16 [16384, 4096], P(('sp', 'tp'))
All inputs are finite; a program needn't handle non-finite values.
Results may differ from a plain program's by a relative error of at most 0.035.
Values may be sent and summed in bfloat16 or wider, within the bound.
No kernel may reach another device: no remote copies, remote signals or barrier semaphores. Data moves between devices by JAX's collectives and lax.ppermute only.
A program may use at most 64 MiB of HBM per device.

v0:
```python
import jax
import jax.numpy as jnp
from jax import lax
from jax.sharding import PartitionSpec as P

HEAD_SIZE = 128
WINDOW_SIDE = 128
GRID_WIDTH = 64


EPS = 1e-05
THETA = 10000.0
MASKED = -1e30


def sent_to_all(value, axis):
    length = lax.axis_size(axis)
    return lax.all_to_all(
        jnp.broadcast_to(value[None], (length, *value.shape)), axis, 0, 0, tiled=True
    )


def taken_together(value, axis):
    everything = sent_to_all(value, axis)
    return jnp.sum(everything, axis=0)


def in_one(arrays, axis):
    line, at, done = (jnp.concatenate([a.reshape(-1) for a in arrays]), 0, [])
    subtotal = taken_together(line, axis)
    for a in arrays:
        done.append(subtotal[at : at + a.size].reshape(a.shape))
        at += a.size
    return tuple(done)


def side_by_side(arrays, axis, dim, along):
    widths = [a.shape[along] for a in arrays]
    both = jnp.concatenate(arrays, axis=along)
    filled = lax.all_gather(both, axis, axis=dim, tiled=True)
    return tuple(jnp.split(filled, [sum(widths[:k]) for k in range(1, len(widths))], axis=along))


def in_order(tiles, dim):
    tiles = jnp.moveaxis(tiles, 0, dim)
    lengths = tiles.shape
    return tiles.reshape(*lengths[:dim], lengths[dim] * lengths[dim + 1], *lengths[dim + 2 :])


def gather_directly(value, axis, dim):
    tiles = sent_to_all(value, axis)
    return in_order(tiles, dim)


def with_halo(cells, sides, width):
    for axis, dim in sides:
        count = lax.axis_size(axis)
        ends = count - 1
        head = lax.slice_in_dim(cells, 0, width, axis=dim)
        tail = lax.slice_in_dim(cells, cells.shape[dim] - width, cells.shape[dim], axis=dim)
        cells = jnp.concatenate(
            [
                lax.ppermute(tail, axis, [(i, (i + 1) % count) for i in range(ends)]),
                cells,
                lax.ppermute(head, axis, [((i + 1) % count, i) for i in range(ends)]),
            ],
            axis=dim,
        )
    return cells


def layer_norm(rows):
    values = rows.astype(jnp.float32)
    mean = jnp.mean(values, axis=-1, keepdims=True)
    var = jnp.mean(jnp.square(values - mean), axis=-1, keepdims=True)
    return (values - mean) * lax.rsqrt(var + EPS)


def rotate_half(values, token_position, width):
    half = width // 2
    inverse = THETA ** (-jnp.arange(half, dtype=jnp.float32) * 2.0 / width)
    angle = token_position.astype(jnp.float32)[:, None] * inverse[None, :]
    cosine = jnp.cos(angle)[:, None, :]
    sine = jnp.sin(angle)[:, None, :]
    first = values[..., :half]
    second = values[..., half:]
    return jnp.concatenate(
        [first * cosine - second * sine, second * cosine + first * sine], axis=-1
    )


def axial_rotation(heads, token_position, grid):
    width = heads.shape[-1] // 2
    values = heads.astype(jnp.float32)
    turned = jnp.concatenate(
        [
            rotate_half(values[..., :width], token_position // grid, width),
            rotate_half(values[..., width:], token_position % grid, width),
        ],
        axis=-1,
    )
    return turned.astype(jnp.bfloat16)


def sink_weights(scores, sink_column):
    top = jnp.maximum(jnp.max(scores, axis=-1, keepdims=True), sink_column)
    expo = jnp.exp(scores - top)
    return (expo / (jnp.sum(expo, axis=-1, keepdims=True) + jnp.exp(sink_column - top))).astype(
        jnp.bfloat16
    )


def shards(
    latent,
    context,
    cond,
    ctx_cond,
    w_shift,
    w_scale,
    w_gate,
    w_query,
    key_weight,
    value_weight,
    w_out,
    sink,
):
    sp_count = lax.axis_size("sp")
    sp_index = lax.axis_index("sp")
    tp_index = lax.axis_index("tp")
    block_rows = w_shift.shape[0]
    act = jax.nn.silu(jnp.stack([cond, ctx_cond])).astype(jnp.bfloat16)
    own_act = lax.dynamic_slice_in_dim(act, sp_index * block_rows, block_rows, 1)
    shift_part = jnp.dot(own_act, w_shift, preferred_element_type=jnp.float32)
    scale_part = jnp.dot(own_act, w_scale, preferred_element_type=jnp.float32)
    gate_part = jnp.dot(own_act[0:1], w_gate, preferred_element_type=jnp.float32)
    shift_sum, scale_sum, gate_sum = in_one((shift_part, scale_part, gate_part), "sp")
    shift, scale, gate = side_by_side((shift_sum, scale_sum, gate_sum), "tp", 1, 0)
    latent_mod = (layer_norm(latent) * (1.0 + scale[0]) + shift[0]).astype(jnp.bfloat16)
    ctx_mod = (layer_norm(context) * (1.0 + scale[1]) + shift[1]).astype(jnp.bfloat16)
    kv_cols = key_weight.shape[1]
    q_cols = w_query.shape[1]
    ctx_pair = gather_directly(
        jnp.concatenate(
            [
                jnp.dot(ctx_mod, key_weight, preferred_element_type=jnp.float32).astype(
                    jnp.bfloat16
                ),
                jnp.dot(ctx_mod, value_weight, preferred_element_type=jnp.float32).astype(
                    jnp.bfloat16
                ),
            ],
            axis=1,
        ),
        "sp",
        0,
    )
    piece = lax.all_gather(latent_mod, "tp", axis=0, tiled=True)
    projected_rows = jnp.concatenate(
        [
            jnp.dot(piece, w_query, preferred_element_type=jnp.float32).astype(jnp.bfloat16),
            jnp.dot(piece, key_weight, preferred_element_type=jnp.float32).astype(jnp.bfloat16),
            jnp.dot(piece, value_weight, preferred_element_type=jnp.float32).astype(jnp.bfloat16),
        ],
        axis=1,
    )
    tokens_here = projected_rows.shape[0]
    kv_heads = kv_cols // HEAD_SIZE
    q_heads = q_cols // HEAD_SIZE
    query_group = q_heads // kv_heads
    offset = sp_index * tokens_here
    token_position = offset + jnp.arange(tokens_here, dtype=jnp.int32)
    query = axial_rotation(
        projected_rows[:, :q_cols].reshape(tokens_here, q_heads, HEAD_SIZE),
        token_position,
        GRID_WIDTH,
    )
    key = axial_rotation(
        projected_rows[:, q_cols : q_cols + kv_cols].reshape(tokens_here, kv_heads, HEAD_SIZE),
        token_position,
        GRID_WIDTH,
    )
    value_rows = projected_rows[:, q_cols + kv_cols :]
    extended = with_halo(
        jnp.concatenate([key.reshape(tokens_here, kv_cols), value_rows], axis=1),
        (("sp", 0),),
        WINDOW_SIDE,
    )
    block_list = tokens_here // WINDOW_SIDE
    band = jnp.concatenate(
        [
            extended[shift_index * WINDOW_SIDE : shift_index * WINDOW_SIDE + tokens_here].reshape(
                block_list, WINDOW_SIDE, 2 * kv_cols
            )
            for shift_index in range(3)
        ],
        axis=1,
    )
    band_key = band[..., :kv_cols].reshape(block_list, 3 * WINDOW_SIDE, kv_heads, HEAD_SIZE)
    band_value = band[..., kv_cols:].reshape(block_list, 3 * WINDOW_SIDE, kv_heads, HEAD_SIZE)
    context_key_rows = ctx_pair[:, :kv_cols].reshape(-1, kv_heads, HEAD_SIZE)
    context_value_rows = ctx_pair[:, kv_cols:].reshape(-1, kv_heads, HEAD_SIZE)
    query_block_list = query.reshape(block_list, WINDOW_SIDE, kv_heads, query_group, HEAD_SIZE)
    factor = HEAD_SIZE ** (-0.5)
    band_scores = (
        jnp.einsum(
            "nqhgd,nkhd->nhgqk", query_block_list, band_key, preferred_element_type=jnp.float32
        )
        * factor
    )
    total = tokens_here * sp_count
    qpos = token_position.reshape(block_list, WINDOW_SIDE)[:, :, None]
    kpos = (
        offset
        - WINDOW_SIDE
        + (jnp.arange(block_list, dtype=jnp.int32) * WINDOW_SIDE)[:, None, None]
        + jnp.arange(3 * WINDOW_SIDE, dtype=jnp.int32)[None, None, :]
    )
    valid = (jnp.abs(kpos - qpos) <= WINDOW_SIDE) & (kpos >= 0) & (kpos < total)
    band_scores = jnp.where(valid[:, None, None], band_scores, MASKED)
    ctx_scores = (
        jnp.einsum(
            "nqhgd,khd->nhgqk",
            query_block_list,
            context_key_rows,
            preferred_element_type=jnp.float32,
        )
        * factor
    )
    own_sink = lax.dynamic_slice_in_dim(sink, tp_index * q_heads, q_heads).reshape(
        kv_heads, query_group
    )[:, :, None, None]
    weights = sink_weights(jnp.concatenate([band_scores, ctx_scores], axis=-1), own_sink)
    attended = jnp.einsum(
        "nhgqk,nkhd->nqhgd",
        weights[..., : 3 * WINDOW_SIDE],
        band_value,
        preferred_element_type=jnp.float32,
    ) + jnp.einsum(
        "nhgqk,khd->nqhgd",
        weights[..., 3 * WINDOW_SIDE :],
        context_value_rows,
        preferred_element_type=jnp.float32,
    )
    attended = attended.astype(jnp.bfloat16).reshape(tokens_here, q_cols)
    projected = lax.psum_scatter(
        jnp.dot(attended, w_out, preferred_element_type=jnp.float32).astype(jnp.bfloat16),
        "tp",
        scatter_dimension=0,
        tiled=True,
    ).astype(jnp.float32)
    return (latent.astype(jnp.float32) + gate[0][None, :] * projected).astype(jnp.bfloat16)


def solution(mesh):
    in_specs = (
        P(("sp", "tp"), None),
        P("sp", None),
        P(),
        P(),
        P("sp", "tp"),
        P("sp", "tp"),
        P("sp", "tp"),
        P(None, "tp"),
        P(None, "tp"),
        P(None, "tp"),
        P("tp", None),
        P(),
    )
    out_specs = P(("sp", "tp"), None)
    return jax.shard_map(shards, mesh=mesh, in_specs=in_specs, out_specs=out_specs, check_vma=False)
```

profile of v0, /device:TPU:8, one launch (start us, length us, event | category | flops | bytes accessed | tf_op | source)
XLA Modules:
  0.0 172.2 jit_solution(11445464485622171272)
XLA Ops:
  6.5 0.9 fusion.49
  7.4 1.1 fusion.50
  8.5 1.0 convolution_bitcast_fusion.1
  9.6 1.0 convolution_bitcast_fusion.2
  10.6 0.9 broadcast_in_dim.12
  11.5 11.7 %all-to-all-start = ((f32[32,1,2560]{2,1,0:T(1,128)}), f32[32,1,2560]{2,1,0:T(1,128)}, u32[]{:S(2)}, u32[]{:S(2)}) async-start(f32[32,1,2560]{2,1,0:T(1,128)} %broadcast_in_dim.12), calls=%async_computation | async-start | bytes 655360 | tf_op jit(solution)/shard_map/all_to_all | solution.py:18
  23.3 1.2 convert_reduce_fusion
  24.6 1.3 fusion.10
  25.9 10.0 %all-to-all-done = f32[32,1,2560]{2,1,0:T(1,128)} async-done(((f32[32,1,2560]{2,1,0:T(1,128)}), f32[32,1,2560]{2,1,0:T(1,128)}, u32[]{:S(2)}, u32[]{:S(2)}) %all-to-all-start) | async-done | bytes 327712 | tf_op jit(solution)/shard_map/all_to_all | solution.py:18
  36.0 1.2 reduce_sum.54
  37.2 13.1 %all_gather.6 = f32[5,4096]{1,0:T(8,128)S(1)} all-gather(f32[5,512]{1,0:T(8,128)S(1)} %pad_maximum_fusion.4), channel_id=1, replica_groups=mesh['sp'=32,'tp'=8] {'tp'}, dimensions={1}, use_global_device_ids=true | all-gather | bytes 92160 | tf_op jit(solution)/shard_map/all_gather | solution.py:40
  50.4 2.1 %fusion.13 = bf16[64,4096]{1,0:T(8,128)(2,1)} fusion(bf16[64,4096]{1,0:T(8,128)(2,1)} %param.12, f32[4096]{0:T(1024)S(1)} %bitcast.140, f32[4096]{0:T(1024)S(1)} %bitcast.141, f32[64]{0:T(128)S(1)} %add_rsqrt_fusion.1, f32[64]{0:T(128)S(1)} %broadcast_multiply_fusion.1), kind=kLoop, calls=%fused_computation.30 | loop fusion | flops 1572864 | bytes 1081856 | tf_op jit(solution)/shard_map/convert_element_type | solution.py:138
  53.8 1.9 %fusion.16 = pred[4,128,384]{1,2,0:T(8,128)(4,1)} fusion(s32[4,128]{1,0:T(4,128)S(1)} %add_add_fusion, s32[4,384]{1,0:T(4,128)S(1)} %iota_add_fusion, pred[4,384]{1,0:T(4,128)(4,1)S(1)} %get-tuple-element.33, pred[4,384]{1,0:T(4,128)(4,1)S(1)} %get-tuple-element.32), kind=kLoop, calls=%fused_computation.36 | loop fusion | flops 983040 | bytes 207872 | tf_op jit(solution)/shard_map/and | solution.py:218
  55.7 1.2 multiply_cosine_fusion.1
  56.9 1.5 convolution_convert_fusion.4
  59.7 5.9 %all-to-all-start.1 = ((bf16[32,32,256]{2,1,0:T(8,128)(2,1)}), bf16[32,32,256]{2,1,0:T(8,128)(2,1)}, u32[]{:S(2)}, u32[]{:S(2)}) async-start(bf16[32,32,256]{2,1,0:T(8,128)(2,1)} %broadcast_in_dim.15), calls=%async_computation.1 | async-start | bytes 1048576 | tf_op jit(solution)/shard_map/all_to_all | solution.py:18
  65.6 17.7 %all-gather.2.cloned.1.call-done = bf16[512,4096]{1,0:T(8,128)(2,1)} async-done(((bf16[64,4096]{1,0:T(8,128)(2,1)}), bf16[512,4096]{1,0:T(8,128)(2,1)}) %all-gather.2.cloned.1.call-update) | async-done | bytes 4194320 | tf_op jit(solution)/shard_map/all_gather | solution.py:157
  83.3 3.7 %fusion.9 = f32[512,1,128]{0,2,1:T(8,128)S(1)} fusion(bf16[512,4096]{1,0:T(8,128)(2,1)} %all-gather.2.cloned.1.call-done, bf16[4096,128]{1,0:T(8,128)(2,1)S(1)} %copy-done.4), kind=kOutput, calls=%fused_computation.22 | convolution fusion | flops 537001984 | bytes 5505024 | tf_op jit(solution)/shard_map/dot_general | solution.py:161
  88.2 3.7 %convolution_convert_fusion.2 = bf16[512,128]{1,0:T(8,128)(2,1)S(1)} fusion(bf16[512,4096]{1,0:T(8,128)(2,1)} %all-gather.2.cloned.1.call-done, bf16[4096,128]{1,0:T(8,128)(2,1)} %param.21), kind=kOutput, calls=%fused_computation.19 | convolution fusion | flops 536936448 | bytes 5373952 | tf_op jit(solution)/shard_map/dot_general | solution.py:162
  92.9 3.4 %collective-permute-start = (bf16[128,256]{1,0:T(8,128)(2,1)}, bf16[128,256]{1,0:T(8,128)(2,1)}, u32[]{:S(2)}, u32[]{:S(2)}) collective-permute-start(bf16[128,256]{1,0:T(8,128)(2,1)} %get-tuple-element.19), channel_id=1, source_target_pairs={{0,8},{8,16},{16,24},{24,32},{32,40},{40,48},{48,56},{56,64},{64,7... | collective-permute-start | bytes 196616 | tf_op jit(solution)/shard_map/ppermute | solution.py:63
  96.3 3.3 %collective-permute-start.1 = (bf16[128,256]{1,0:T(8,128)(2,1)}, bf16[128,256]{1,0:T(8,128)(2,1)}, u32[]{:S(2)}, u32[]{:S(2)}) collective-permute-start(bf16[128,256]{1,0:T(8,128)(2,1)} %get-tuple-element.20), channel_id=1, source_target_pairs={{8,0},{16,8},{24,16},{32,24},{40,32},{48,40},{56,48},{64,56},{72,6... | collective-permute-start | bytes 196616 | tf_op jit(solution)/shard_map/ppermute | solution.py:65
  99.7 4.2 %convolution_convert_fusion.1 = bf16[512,256]{0,1:T(8,128)(2,1)S(1)} fusion(bf16[512,4096]{1,0:T(8,128)(2,1)} %all-gather.2.cloned.1.call-done, bf16[4096,256]{1,0:T(8,128)(2,1)} %param.19), kind=kOutput, calls=%fused_computation.17 | convolution fusion | flops 1073872896 | bytes 6553600 | tf_op jit(solution)/shard_map/dot_general | solution.py:160
  105.3 1.0 copy.68
  106.4 1.1 pad_maximum_fusion.3
  107.5 4.3 %fusion.59 = (f32[4,2,128]{2,1,0:T(2,128)}, f32[4,1,2,128,1024]{3,4,2,0,1:T(8,128)}) fusion(bf16[4,128,2,128]{3,1,2,0:T(8,128)(2,1)} %pad_maximum_fusion.3, bf16[1024,256]{1,0:T(8,128)(2,1)} %bitcast.31), kind=kOutput, calls=%fused_computation.123 | convolution fusion | flops 270531584 | bytes 4722688 | tf_op jit(solution)/shard_map/nqhgd,khd->nhgqk/dot_general | solution.py:221
  112.6 1.1 pad_maximum_fusion.2
  113.8 1.5 fusion.58
  116.2 1.0 divide_convert_fusion
  117.5 1.4 fusion.7
  119.2 3.2 %convolution_convert_fusion = bf16[512,4096]{1,0:T(8,128)(2,1)} fusion(bf16[256,4096]{1,0:T(8,128)(2,1)S(1)} %copy-done, bf16[64,8,2,128]{3,2,1,0:T(2,128)(2,1)S(1)} %bitcast.122), kind=kOutput, calls=%fused_computation | convolution fusion | flops 1075838976 | bytes 6553600 | tf_op jit(solution)/shard_map/dot_general | solution.py:246
  122.4 40.9 %reduce-scatter.2.cloned.1.call-done = bf16[64,4096]{1,0:T(8,128)(2,1)} async-done(((bf16[512,4096]{1,0:T(8,128)(2,1)}), bf16[64,4096]{1,0:T(8,128)(2,1)}) %reduce-scatter.2.cloned.1.call-update) | async-done | bytes 524304 | tf_op jit(solution)/shard_map/reduce_scatter | solution.py:245
  163.4 2.0 %fusion.14 = bf16[64,4096]{1,0:T(8,128)(2,1)} fusion(bf16[64,4096]{1,0:T(8,128)(2,1)S(1)} %copy-done.2, bf16[64,4096]{1,0:T(8,128)(2,1)} %reduce-scatter.2.cloned.1.call-done, f32[4096]{0:T(1024)S(1)} %bitcast.139), kind=kLoop, calls=%fused_computation.31 | loop fusion | flops 1310720 | bytes 1589248 | tf_op jit(solution)/shard_map/convert_element_type | solution.py:251
  (101 shorter events, 8.5 us)
Async XLA Ops:
  6.5 112.6 %copy-start = (bf16[256,4096]{1,0:T(8,128)(2,1)S(1)}, bf16[256,4096]{1,0:T(8,128)(2,1)}, u32[]{:S(2)}) copy-start(bf16[256,4096]{1,0:T(8,128)(2,1)} %param.22) | copy-start | bytes 6291460
  6.5 46.0 %copy-start.20 = (f32[16]{0:T(128)S(1)}, f32[16]{0:T(128)}, u32[]{:S(2)}) copy-start(f32[16]{0:T(128)} %param.23) | copy-start | bytes 196
  6.5 46.7 %copy-start.3 = (bf16[32,4096]{1,0:T(8,128)(2,1)S(1)}, bf16[32,4096]{1,0:T(8,128)(2,1)}, u32[]{:S(2)}) copy-start(bf16[32,4096]{1,0:T(8,128)(2,1)} %param.13) | copy-start | bytes 786436
  6.5 51.9 %copy-start.4 = (bf16[4096,128]{1,0:T(8,128)(2,1)S(1)}, bf16[4096,128]{1,0:T(8,128)(2,1)}, u32[]{:S(2)}) copy-start(bf16[4096,128]{1,0:T(8,128)(2,1)} %param.20) | copy-start | bytes 3145732
  11.5 24.4 %all-to-all-start = ((f32[32,1,2560]{2,1,0:T(1,128)}), f32[32,1,2560]{2,1,0:T(1,128)}, u32[]{:S(2)}, u32[]{:S(2)}) async-start(f32[32,1,2560]{2,1,0:T(1,128)} %broadcast_in_dim.12), calls=%async_computation | async-start | bytes 655360 | tf_op jit(solution)/shard_map/all_to_all | solution.py:18
  23.3 60.0 %all-gather.2.cloned.1.call-start = ((), (), s32[]{:S(2)}) async-start(), calls=%async_computation.3 | async-start | bytes 4718592 | tf_op jit(solution)/shard_map/all_gather | solution.py:157
  59.7 47.8 %all-to-all-start.1 = ((bf16[32,32,256]{2,1,0:T(8,128)(2,1)}), bf16[32,32,256]{2,1,0:T(8,128)(2,1)}, u32[]{:S(2)}, u32[]{:S(2)}) async-start(bf16[32,32,256]{2,1,0:T(8,128)(2,1)} %broadcast_in_dim.15), calls=%async_computation.1 | async-start | bytes 1048576 | tf_op jit(solution)/shard_map/all_to_all | solution.py:18
  65.6 97.8 %reduce-scatter.2.cloned.1.call-start = ((), (), s32[]{:S(2)}) async-start(), calls=%async_computation.4 | async-start | bytes 4718592 | tf_op jit(solution)/shard_map/reduce_scatter | solution.py:245
  87.6 0.6 copy-start.6
  87.6 0.6 copy-start.8
  87.6 0.6 copy-start.10
  87.6 0.6 copy-start.12
  92.9 19.7 %collective-permute-start = (bf16[128,256]{1,0:T(8,128)(2,1)}, bf16[128,256]{1,0:T(8,128)(2,1)}, u32[]{:S(2)}, u32[]{:S(2)}) collective-permute-start(bf16[128,256]{1,0:T(8,128)(2,1)} %get-tuple-element.19), channel_id=1, source_target_pairs={{0,8},{8,16},{16,24},{24,32},{32,40},{40,48},{48,56},{56,64},{64,7... | collective-permute-start | bytes 196616 | tf_op jit(solution)/shard_map/ppermute | solution.py:63
  96.3 7.6 %copy-start.14 = (f32[512,32]{0,1:T(8,128)S(1)}, f32[512,32]{0,1:T(8,128)}, u32[]{:S(2)}) copy-start(f32[512,32]{0,1:T(8,128)} %get-tuple-element.28) | copy-start | bytes 196612
  96.3 7.6 %copy-start.15 = (f32[512,32]{0,1:T(8,128)S(1)}, f32[512,32]{0,1:T(8,128)}, u32[]{:S(2)}) copy-start(f32[512,32]{0,1:T(8,128)} %get-tuple-element.29) | copy-start | bytes 196612
  96.3 7.6 %copy-start.16 = (f32[512,32]{0,1:T(8,128)S(1)}, f32[512,32]{0,1:T(8,128)}, u32[]{:S(2)}) copy-start(f32[512,32]{0,1:T(8,128)} %get-tuple-element.34) | copy-start | bytes 196612
  96.3 7.6 %copy-start.17 = (f32[512,32]{0,1:T(8,128)S(1)}, f32[512,32]{0,1:T(8,128)}, u32[]{:S(2)}) copy-start(f32[512,32]{0,1:T(8,128)} %get-tuple-element.35) | copy-start | bytes 196612
  96.3 16.3 %collective-permute-start.1 = (bf16[128,256]{1,0:T(8,128)(2,1)}, bf16[128,256]{1,0:T(8,128)(2,1)}, u32[]{:S(2)}, u32[]{:S(2)}) collective-permute-start(bf16[128,256]{1,0:T(8,128)(2,1)} %get-tuple-element.20), channel_id=1, source_target_pairs={{8,0},{16,8},{24,16},{32,24},{40,32},{48,40},{56,48},{64,56},{72,6... | collective-permute-start | bytes 196616 | tf_op jit(solution)/shard_map/ppermute | solution.py:65
  107.4 4.4 %copy-start.13 = (bf16[512,1,32]{0,2,1:T(8,128)(2,1)S(1)}, bf16[512,1,32]{0,2,1:T(8,128)(2,1)}, u32[]{:S(2)}) copy-start(bf16[512,1,32]{0,2,1:T(8,128)(2,1)} %copy-done.12) | copy-start | bytes 98308
  107.4 4.5 %copy-start.11 = (bf16[512,1,32]{0,2,1:T(8,128)(2,1)S(1)}, bf16[512,1,32]{0,2,1:T(8,128)(2,1)}, u32[]{:S(2)}) copy-start(bf16[512,1,32]{0,2,1:T(8,128)(2,1)} %copy-done.10) | copy-start | bytes 98308
  107.4 4.6 %copy-start.9 = (bf16[512,1,32]{0,2,1:T(8,128)(2,1)S(1)}, bf16[512,1,32]{0,2,1:T(8,128)(2,1)}, u32[]{:S(2)}) copy-start(bf16[512,1,32]{0,2,1:T(8,128)(2,1)} %copy-done.8) | copy-start | bytes 98308
  107.4 4.8 %copy-start.7 = (bf16[512,1,32]{0,2,1:T(8,128)(2,1)S(1)}, bf16[512,1,32]{0,2,1:T(8,128)(2,1)}, u32[]{:S(2)}) copy-start(bf16[512,1,32]{0,2,1:T(8,128)(2,1)} %copy-done.6) | copy-start | bytes 98308
  107.4 6.3 %copy-start.5 = (bf16[4,128,2,128]{3,1,2,0:T(8,128)(2,1)S(1)}, bf16[4,128,2,128]{3,1,2,0:T(8,128)(2,1)}, u32[]{:S(2)}) copy-start(bf16[4,128,2,128]{3,1,2,0:T(8,128)(2,1)} %pad_maximum_fusion.3) | copy-start | bytes 786436
  112.6 2.7 %copy-start.18 = (f32[4,2,128]{2,1,0:T(2,128)S(1)}, f32[4,2,128]{2,1,0:T(2,128)}, u32[]{:S(2)}) copy-start(f32[4,2,128]{2,1,0:T(2,128)} %get-tuple-element.38) | copy-start | bytes 12292
  112.6 2.7 %copy-start.19 = (f32[2]{0:T(128)S(1)}, f32[2]{0:T(128)}, u32[]{:S(2)}) copy-start(f32[2]{0:T(128)} %dynamic_slice.7) | copy-start | bytes 28
  112.6 2.7 %copy-start.1 = (f32[4,1,2,128,1024]{3,4,2,0,1:T(8,128)S(1)}, f32[4,1,2,128,1024]{3,4,2,0,1:T(8,128)}, u32[]{:S(2)}) copy-start(f32[4,1,2,128,1024]{3,4,2,0,1:T(8,128)} %get-tuple-element.39) | copy-start | bytes 12582916
  119.2 44.2 %copy-start.2 = (bf16[64,4096]{1,0:T(8,128)(2,1)S(1)}, bf16[64,4096]{1,0:T(8,128)(2,1)}, u32[]{:S(2)}) copy-start(bf16[64,4096]{1,0:T(8,128)(2,1)} %param.12) | copy-start | bytes 1572868
Sparse Core Ops, SparseCore 0:
  52.6 30.6 all-gather.1
  122.5 40.7 reduce-scatter.1
where the time goes:
time: 173 us; the launch traced here: 172 us
  waiting for transfers between devices  68.7 us (40%)
  matrix products  27.4 us (16%)
  starting transfers between devices  24.4 us (14%)
  other arithmetic  17.3 us (10%)
  between operations  14 us (8%)
  blocking collectives  13.1 us (8%)
  local copies, waits for them, and re-layouts  7.21 us (4%)
    reduce_scatter x1, waiting for transfers between devices, shards(): lax.psum_scatter(jnp.dot(attended, w_out, preferred_element_type=jnp.floa...  40.9 us
    all_gather x1, waiting for transfers between devices, shards(): piece = lax.all_gather(latent_mod, 'tp', axis=0, tiled=True)  17.7 us
    all_to_all x2, starting transfers between devices, sent_to_all(): lax.all_to_all(jnp.broadcast_to(value[None], (length, *value.shape)), axi...  17.6 us
    all_gather x1, blocking collectives, side_by_side(): filled = lax.all_gather(both, axis, axis=dim, tiled=True)  13.1 us
    all_to_all x2, waiting for transfers between devices, sent_to_all(): lax.all_to_all(jnp.broadcast_to(value[None], (length, *value.shape)), axi...  10 us
    dot_general x1, matrix products, shards(): jnp.einsum('nqhgd,khd->nhgqk', query_block_list, context_key_rows, prefer...  4.34 us
    dot_general x1, matrix products, shards(): jnp.dot(piece, w_query, preferred_element_type=jnp.float32)  4.16 us
    dot_general x1, matrix products, shards(): jnp.dot(piece, value_weight, preferred_element_type=jnp.float32)  3.73 us
  transfers between devices with their start and end apart: 6, of which 3 were waited for; matrix products, arithmetic and copies ran while one was open for 18% of the time, Pallas kernels for 0%

commit v1 on v0

v1 whole, which is shorter than its diff:
```python
import functools

import jax
import jax.numpy as jnp
from jax import lax
from jax.experimental import pallas as pl
from jax.experimental.pallas import tpu as pltpu
from jax.sharding import PartitionSpec as P

HEAD = 128
SIDE = 128
GRID_WIDTH = 64
EPS = 1e-05
THETA = 10000.0
MASKED = -1e30
LOG2E = 1.4426950408889634

F32 = jnp.float32
BF16 = jnp.bfloat16
ANY = pl.BlockSpec(memory_space=pl.ANY)
VMEM = pl.BlockSpec(memory_space=pltpu.VMEM)
SMEM = pl.BlockSpec(memory_space=pltpu.SMEM)


def cost(flops, moved):
    return pl.CostEstimate(flops=int(flops), bytes_accessed=int(moved), transcendentals=0)


def params(mib=48):
    return pltpu.CompilerParams(vmem_limit_bytes=mib * 1024 * 1024)


def dot(a, b):
    return jnp.dot(a, b, preferred_element_type=F32)


def dot_nt(a, b):
    return lax.dot_general(a, b, (((1,), (1,)), ((), ())), preferred_element_type=F32)


def modulation_part(index, cond, ctx_cond, w_shift, w_scale, w_gate, count):
    rows, cols = w_shift.shape

    def kernel(index_ref, cond_ref, ctx_ref, shift_ref, scale_ref, gate_ref, out_ref):
        own = pl.ds(index_ref[0], 1)
        first = cond_ref[own, :]
        second = ctx_ref[own, :]
        line = lax.broadcasted_iota(jnp.int32, (8, rows), 0)
        both = jnp.where(line == 0, first, jnp.where(line == 1, second, 0.0))
        act = (both / (1.0 + jnp.exp(-both))).astype(BF16)
        shift = dot(act, shift_ref[...])
        scale = dot(act, scale_ref[...])
        gate = dot(act, gate_ref[...])
        part = jnp.concatenate([shift[0:2], scale[0:2], gate[0:1], jnp.zeros((3, cols), F32)], axis=0)
        part = part.astype(BF16)
        for k in range(count):
            out_ref[k] = part

    return pl.pallas_call(
        kernel,
        out_shape=jax.ShapeDtypeStruct((count, 8, cols), BF16),
        in_specs=[SMEM] + [VMEM] * 5,
        out_specs=VMEM,
        compiler_params=params(),
        cost_estimate=cost(3 * 2 * 8 * rows * cols * 20, 3 * rows * cols * 2),
        name="modulation_part",
    )(index, cond.reshape(-1, rows), ctx_cond.reshape(-1, rows), w_shift, w_scale, w_gate)


def modulation_sum(parts, copies):
    count, rows, cols = parts.shape

    def kernel(parts_ref, out_ref):
        total = jnp.sum(parts_ref[...].astype(F32), axis=0)
        for k in range(copies):
            out_ref[k] = total

    return pl.pallas_call(
        kernel,
        out_shape=jax.ShapeDtypeStruct((copies, rows, cols), F32),
        in_specs=[VMEM],
        out_specs=VMEM,
        compiler_params=params(),
        cost_estimate=cost(1e7, count * rows * cols * 2),
        name="modulation_sum",
    )(parts)


def row_of(mod_ref, line):
    return jnp.concatenate([mod_ref[t, line : line + 1, :] for t in range(mod_ref.shape[0])], axis=1)


def normed(x, scale, shift):
    mean = jnp.mean(x, axis=-1, keepdims=True)
    centred = x - mean
    var = jnp.mean(centred * centred, axis=-1, keepdims=True)
    return (centred * lax.rsqrt(var + EPS) * (1.0 + scale) + shift).astype(BF16)


def context_pairs(context, mod, key_weight, value_weight, count):
    tokens, width = context.shape
    cols = key_weight.shape[1]

    def kernel(ctx_ref, mod_ref, key_ref, value_ref, out_ref):
        rows = normed(ctx_ref[...].astype(F32), row_of(mod_ref, 3), row_of(mod_ref, 1))
        pair = jnp.concatenate([dot(rows, key_ref[...]), dot(rows, value_ref[...])], axis=1).astype(BF16)
        for k in range(count):
            out_ref[k] = pair

    return pl.pallas_call(
        kernel,
        out_shape=jax.ShapeDtypeStruct((count, tokens, 2 * cols), BF16),
        in_specs=[VMEM] * 4,
        out_specs=VMEM,
        compiler_params=params(),
        cost_estimate=cost(2e9, 3e6),
        name="context_pairs",
    )(context, mod, key_weight, value_weight)


def rotary_tables(position):
    lane = jnp.arange(HEAD, dtype=jnp.int32)
    width = HEAD // 2
    inverse = THETA ** (-(lane % (width // 2)).astype(F32) * 2.0 / width)
    row = (position // GRID_WIDTH).astype(F32)
    col = (position % GRID_WIDTH).astype(F32)
    angle = jnp.where(lane[None, :] < width, row[:, None], col[:, None]) * inverse[None, :]
    sign = jnp.where(lane % width < width // 2, -1.0, 1.0).astype(F32)
    return jnp.cos(angle), jnp.sin(angle) * sign[None, :]


def turned(x, cosine, sine):
    x = x.astype(BF16).astype(F32)
    quarter = HEAD // 4
    lane = lax.broadcasted_iota(jnp.int32, x.shape, 1)
    other = jnp.where(
        lane % (2 * quarter) < quarter,
        pltpu.roll(x, HEAD - quarter, 1),
        pltpu.roll(x, quarter, 1),
    )
    return (x * cosine + other * sine).astype(BF16)


def projections(place, pieces, mod, w_query, key_weight, value_weight, cosine, sine):
    width = w_query.shape[0]
    q_cols, kv_cols = w_query.shape[1], key_weight.shape[1]
    flat, where = [], []
    chips = len(pieces)
    for r, sides in enumerate(pieces):
        for side, parts in enumerate(sides):
            at = 0
            for part in parts:
                flat.append(part)
                where.append((r, side, at, part.shape[0]))
                at += part.shape[0]
            half = at
    block = 2 * half
    tokens = chips * block
    n = len(flat)

    def kernel(place_ref, *refs):
        part_refs = refs[:n]
        mod_ref, q_w, k_w, v_w, cos_ref, sin_ref = refs[n : n + 6]
        q_out, kv_out, head_out, tail_out = refs[n + 6 : n + 10]
        x_ref, wq_ref, wk_ref, wv_ref, part_sems, weight_sems = refs[n + 10 :]
        chip, core = place_ref[1], place_ref[2]
        weights = [
            pltpu.make_async_copy(source, target, weight_sems.at[k])
            for k, (source, target) in enumerate(((k_w, wk_ref), (v_w, wv_ref), (q_w, wq_ref)))
        ]
        copies = []
        for k, (r, side, at, length) in enumerate(where):
            to = core if side == 0 else 1 - core
            copies.append(
                pltpu.make_async_copy(part_refs[k], x_ref.at[r, to, pl.ds(at, length)], part_sems.at[k])
            )
        for k, copy in enumerate(copies):
            if where[k][0] == 0:
                copy.start()
        for copy in weights:
            copy.start()
        for k, copy in enumerate(copies):
            if where[k][0] != 0:
                copy.start()
        scale, shift = row_of(mod_ref, 2), row_of(mod_ref, 0)
        for r in range(chips):
            for k, copy in enumerate(copies):
                if where[k][0] == r:
                    copy.wait()
            rows = normed(x_ref[r].reshape(block, width).astype(F32), scale, shift)
            if r == 0:
                for copy in weights:
                    copy.wait()
            place_of = lax.rem(chip + r, chips)
            at = pl.ds(pl.multiple_of(place_of * block, block), block)
            cos, sin = cos_ref[at, :], sin_ref[at, :]
            key = turned(dot(rows, wk_ref[...]), cos, sin)
            value = dot(rows, wv_ref[...]).astype(BF16)
            pair = jnp.concatenate([key, value], axis=1)
            kv_out[at, :] = pair

            @pl.when(place_of == 0)
            def _():
                head_out[...] = pair

            @pl.when(place_of == chips - 1)
            def _():
                tail_out[...] = pair

            query = dot(rows, wq_ref[...])
            for h in range(q_cols // HEAD):
                q_out[at, h * HEAD : (h + 1) * HEAD] = turned(query[:, h * HEAD : (h + 1) * HEAD], cos, sin)

    return pl.pallas_call(
        kernel,
        out_shape=(
            jax.ShapeDtypeStruct((tokens, q_cols), BF16),
            jax.ShapeDtypeStruct((tokens, 2 * kv_cols), BF16),
            jax.ShapeDtypeStruct((block, 2 * kv_cols), BF16),
            jax.ShapeDtypeStruct((block, 2 * kv_cols), BF16),
        ),
        in_specs=[SMEM] + [ANY] * n + [VMEM] + [ANY] * 3 + [VMEM] * 2,
        out_specs=(VMEM,) * 4,
        scratch_shapes=[
            pltpu.VMEM((chips, 2, half, width), BF16),
            pltpu.VMEM((width, q_cols), BF16),
            pltpu.VMEM((width, kv_cols), BF16),
            pltpu.VMEM((width, kv_cols), BF16),
            pltpu.SemaphoreType.DMA((n,)),
            pltpu.SemaphoreType.DMA((3,)),
        ],
        compiler_params=params(),
        cost_estimate=cost(8e9, 8e6),
        name="projections",
    )(place, *flat, mod, w_query, key_weight, value_weight, cosine, sine)


def attention(place, order, query, pairs, before, after, ctx_pairs, sink, chips, total):
    tokens, q_cols = query.shape
    block = tokens // chips
    half = block // 2
    heads = q_cols // HEAD
    kv_cols = pairs.shape[1] // 2
    ctx_tokens = ctx_pairs.shape[0]
    n = len(order)
    factor = LOG2E * HEAD**-0.5

    def kernel(place_ref, sink_ref, q_ref, kv_ref, before_ref, after_ref, ctx_ref, mine_out, other_out, ext_ref, sems):
        sp, chip, core = place_ref[0], place_ref[1], place_ref[2]
        copies = [
            pltpu.make_async_copy(before_ref, ext_ref.at[pl.ds(0, SIDE)], sems.at[0]),
            pltpu.make_async_copy(kv_ref, ext_ref.at[pl.ds(SIDE, tokens)], sems.at[1]),
            pltpu.make_async_copy(after_ref, ext_ref.at[pl.ds(SIDE + tokens, SIDE)], sems.at[2]),
        ]
        for copy in copies:
            copy.start()
        for copy in copies:
            copy.wait()
        ctx_key = ctx_ref[:, :kv_cols]
        ctx_value = ctx_ref[:, kv_cols:]
        rows = heads * block
        i = lax.rem(lax.broadcasted_iota(jnp.int32, (rows, 3 * SIDE), 0), block)
        j = lax.broadcasted_iota(jnp.int32, (rows, 3 * SIDE), 1)
        line = lax.broadcasted_iota(jnp.int32, (rows, 1), 0)
        sink_column = jnp.zeros((rows, 1), F32)
        for h in range(heads):
            sink_column = jnp.where(line // block == h, sink_ref[place_ref[3] + h] * LOG2E, sink_column)
        for k, r in enumerate(order):
            place_of = lax.rem(chip + r, chips)
            at = pl.multiple_of(place_of * block, block)
            q = q_ref[pl.ds(at, block), :]
            q = jnp.concatenate([q[:, h * HEAD : (h + 1) * HEAD] for h in range(heads)], axis=0)
            window = pl.ds(at, 3 * SIDE)
            position = sp * tokens + at - SIDE + j
            valid = (j >= i) & (j <= i + 2 * SIDE) & (position >= 0) & (position < total)
            near = jnp.where(valid, dot_nt(q, ext_ref[window, :kv_cols]) * factor, MASKED)
            far = dot_nt(q, ctx_key) * factor
            top = jnp.maximum(
                jnp.maximum(jnp.max(near, axis=-1, keepdims=True), jnp.max(far, axis=-1, keepdims=True)),
                sink_column,
            )
            near = jnp.exp2(near - top)
            far = jnp.exp2(far - top)
            whole = (
                jnp.sum(near, axis=-1, keepdims=True)
                + jnp.sum(far, axis=-1, keepdims=True)
                + jnp.exp2(sink_column - top)
            )
            out = dot(near.astype(BF16), ext_ref[window, kv_cols:]) + dot(far.astype(BF16), ctx_value)
            out = (out / whole).astype(BF16)
            out = jnp.concatenate([out[h * block : (h + 1) * block] for h in range(heads)], axis=1)
            south, north = out[:half], out[half:]
            mine_out[k * half : (k + 1) * half] = jnp.where(core == 0, south, north)
            other_out[k * half : (k + 1) * half] = jnp.where(core == 0, north, south)

    return pl.pallas_call(
        kernel,
        out_shape=(jax.ShapeDtypeStruct((n * half, q_cols), BF16),) * 2,
        in_specs=[SMEM, SMEM, VMEM, ANY, ANY, ANY, VMEM],
        out_specs=(VMEM,) * 2,
        scratch_shapes=[pltpu.VMEM((tokens + 2 * SIDE, 2 * kv_cols), BF16), pltpu.SemaphoreType.DMA((3,))],
        compiler_params=params(),
        cost_estimate=cost(n * 1.5e9, 2e6),
        name=f"attention_{n}",
    )(place, sink, query, pairs, before, after, ctx_pairs)


def out_projection(mine, other, w_mine, w_other, cuts, types):
    rows, depth = mine.shape
    width = w_mine.shape[1]
    tile = 512

    def kernel(mine_ref, other_ref, w_mine_ref, w_other_ref, *outs):
        total = dot(mine_ref[...], w_mine_ref[...]) + dot(other_ref[...], w_other_ref[...])
        at = 0
        for out, length in zip(outs, cuts):
            out[...] = total[at : at + length].astype(out.dtype)
            at += length

    return pl.pallas_call(
        kernel,
        grid=(width // tile,),
        out_shape=tuple(jax.ShapeDtypeStruct((c, width), t) for c, t in zip(cuts, types)),
        in_specs=[pl.BlockSpec((rows, depth), lambda k: (0, 0))] * 2
        + [pl.BlockSpec((depth, tile), lambda k: (0, k))] * 2,
        out_specs=tuple(pl.BlockSpec((c, tile), lambda k: (0, k)) for c in cuts),
        compiler_params=params(),
        cost_estimate=cost(2 * rows * 2 * depth * width * 4, 4e6),
        name=f"out_projection_{rows}",
    )(mine, other, w_mine, w_other)


def shards(
    latent,
    context,
    cond,
    ctx_cond,
    w_shift,
    w_scale,
    w_gate,
    w_query,
    key_weight,
    value_weight,
    w_out,
    sink,
):
    sp_count = lax.axis_size("sp")
    tp_count = lax.axis_size("tp")
    sp = lax.axis_index("sp")
    tp = lax.axis_index("tp")
    chips = tp_count // 2
    q_heads = w_query.shape[1] // HEAD
    place = jnp.stack([sp, tp // 2, tp % 2, tp * q_heads]).astype(jnp.int32)
    to_right = [(i, (i + 2) % tp_count) for i in range(tp_count)]
    to_left = [(i, (i - 2) % tp_count) for i in range(tp_count)]
    swap = [(i, i ^ 1) for i in range(tp_count)]

    def right(v):
        return lax.ppermute(v, "tp", to_right)

    def left(v):
        return lax.ppermute(v, "tp", to_left)

    def across(v):
        return lax.ppermute(v, "tp", swap)

    half = latent.shape[0]
    cut = half // 2
    from_left = right(latent)
    from_right = left(latent)
    own_other = across(latent)

    parts = modulation_part(place, cond, ctx_cond, w_shift, w_scale, w_gate, sp_count)
    parts = lax.all_to_all(parts, "sp", 0, 0, tiled=True)
    w_out_other = across(w_out)

    far_a = right(from_left[:cut])
    far_b = left(from_right[cut:])
    left_other = across(from_left)
    right_other = across(from_right)

    mod = lax.all_to_all(modulation_sum(parts, tp_count), "tp", 0, 0, tiled=True)
    far_a_other = across(far_a)
    far_b_other = across(far_b)

    ctx_pairs = context_pairs(context, mod, key_weight, value_weight, sp_count)
    ctx_pairs = lax.all_to_all(ctx_pairs, "sp", 0, 0, tiled=True)
    ctx_pairs = ctx_pairs.reshape(-1, ctx_pairs.shape[-1])

    tokens = half * tp_count
    position = sp * tokens + jnp.arange(tokens, dtype=jnp.int32)
    cosine, sine = rotary_tables(position)
    pieces = [
        ((latent,), (own_other,)),
        ((from_right,), (right_other,)),
        ((far_a, far_b), (far_a_other, far_b_other)),
        ((from_left,), (left_other,)),
    ]
    query, pairs, first, last = projections(
        place, pieces, mod, w_query, key_weight, value_weight, cosine, sine
    )
    before = lax.ppermute(last, "sp", [(i, i + 1) for i in range(sp_count - 1)])
    after = lax.ppermute(first, "sp", [(i + 1, i) for i in range(sp_count - 1)])

    attend = functools.partial(
        attention,
        query=query,
        pairs=pairs,
        before=before,
        after=after,
        ctx_pairs=ctx_pairs,
        sink=sink,
        chips=chips,
        total=tokens * sp_count,
    )
    far_mine, far_away = attend(place, (2,))
    far_got = across(far_away)
    rest_mine, rest_away = attend(place, (1, 3, 0))
    rest_got = across(rest_away)
    send_a, send_b = out_projection(far_mine, far_got, w_out, w_out_other, (cut, cut), (BF16,) * 2)
    hop_a = right(send_a)
    hop_b = left(send_b)
    right_a, right_b, left_a, left_b, own = out_projection(
        rest_mine, rest_got, w_out, w_out_other, (cut,) * 4 + (half,), (BF16,) * 4 + (F32,)
    )
    got_left_b = right(right_b)
    got_right_a = left(left_a)
    got_left_a = right((right_a.astype(F32) + hop_a.astype(F32)).astype(BF16))
    got_right_b = left((left_b.astype(F32) + hop_b.astype(F32)).astype(BF16))
    gate = mod[:, 4, :].reshape(1, -1)
    projected = own + jnp.concatenate(
        [
            got_left_a.astype(F32) + got_right_a.astype(F32),
            got_left_b.astype(F32) + got_right_b.astype(F32),
        ],
        axis=0,
    )
    return (latent.astype(F32) + gate * projected).astype(BF16)


def solution(mesh):
    in_specs = (
        P(("sp", "tp"), None),
        P("sp", None),
        P(),
        P(),
        P("sp", "tp"),
        P("sp", "tp"),
        P("sp", "tp"),
        P(None, "tp"),
        P(None, "tp"),
        P(None, "tp"),
        P("tp", None),
        P(),
    )
    out_specs = P(("sp", "tp"), None)
    return jax.shard_map(shards, mesh=mesh, in_specs=in_specs, out_specs=out_specs, check_vma=False)
```

time: 173 us -> 121 us (0.70)
  the two profiles are of different devices: /device:TPU:8 before, /device:TPU:38 now
where the time goes in v1:
time: 121 us; the launch traced here: 120 us
  starting transfers between devices  42.6 us (35%)
  waiting for transfers between devices  31.5 us (26%)
  Pallas kernels  28.1 us (23%)
  local copies, waits for them, and re-layouts  15.1 us (12%)
  other arithmetic  2.31 us (2%)
    ppermute x5, waiting for transfers between devices, left(): return lax.ppermute(v, 'tp', to_left)  17.6 us
    pallas_call x1, Pallas kernels, projections(): pl.pallas_call(kernel, out_shape=(jax.ShapeDtypeStruct((tokens, q_cols),...  12.3 us
    unnamed x36, local copies, waits for them, and re-layouts  11.7 us
    all_to_all x1, starting transfers between devices, shards(): parts = lax.all_to_all(parts, 'sp', 0, 0, tiled=True)  11.4 us
    ppermute x5, starting transfers between devices, right(): return lax.ppermute(v, 'tp', to_right)  9.47 us
    pallas_call x2, Pallas kernels, out_projection(): pl.pallas_call(kernel, grid=(width // tile,), out_shape=tuple((jax.ShapeD...  7.6 us
    ppermute x1, waiting for transfers between devices, shards(): before = lax.ppermute(last, 'sp', [(i, i + 1) for i in range(sp_count - 1)])  6.31 us
    all_to_all x1, waiting for transfers between devices, shards(): parts = lax.all_to_all(parts, 'sp', 0, 0, tiled=True)  5.57 us
  transfers between devices with their start and end apart: 23, of which 5 were waited for; matrix products, arithmetic and copies ran while one was open for 4% of the time, Pallas kernels for 23%

profile of v1, /device:TPU:38, one launch (start us, length us, event | category | flops | bytes accessed | tf_op | source)
XLA Modules:
  0.0 120.0 jit_solution(3312421402885333550)
XLA Ops:
  0.5 1.5 %collective-permute-start.1 = (bf16[64,4096]{1,0:T(8,128)(2,1)}, bf16[64,4096]{1,0:T(8,128)(2,1)}, u32[]{:S(2)}, u32[]{:S(2)}) collective-permute-start(bf16[64,4096]{1,0:T(8,128)(2,1)} %refs_0_.1), channel_id=1, source_target_pairs={{0,6},{1,7},{2,0},{3,1},{4,2},{5,3},{6,4},{7,5},{8,14},{9,15},{10,... | collective-permute-start | bytes 1572872 | tf_op jit(solution)/shard_map/ppermute | solution.py:362
  2.1 0.9 copy-done.3
  6.3 1.4 %modulation_part.1 = bf16[32,8,512]{2,1,0:T(8,128)(2,1)} custom-call(s32[4]{0:T(128)S(1)} %pad_add_fusion.index_ref.place_ref, f32[32,128]{1,0:T(8,128)S(1)} %bitcast.10, f32[32,128]{1,0:T(8,128)S(1)} %bitcast.11, bf16[128,512]{1,0:T(8,128)(2,1)S(1)} %copy-done.3, bf16[128,512]{1,0:T(8,128)(2,1)S(1)} %copy-done.4, bf16[128,512]{1,0:T(8,128)(2,1)S(1)} %copy-done.5), custom_call_target="tpu_custom_call" | custom-call | flops 62914560 | bytes 393216 | tf_op jit(solution)/shard_map/modulation_part/pallas_call | solution.py:59
  7.7 11.4 %all-to-all-start = ((bf16[32,8,512]{2,1,0:T(8,128)(2,1)}), bf16[32,8,512]{2,1,0:T(8,128)(2,1)S(1)}, u32[]{:S(2)}, u32[]{:S(2)}) async-start(bf16[32,8,512]{2,1,0:T(8,128)(2,1)} %modulation_part.1), calls=%async_computation | async-start | bytes 524288 | tf_op jit(solution)/shard_map/all_to_all | solution.py:374
  19.7 1.7 %slice.13 = bf16[32,4096]{1,0:T(8,128)(2,1)} slice(bf16[64,4096]{1,0:T(8,128)(2,1)} %collective-permute-done.3.refs_8_), slice={[0:32], [0:4096]} | slice | bytes 524288 | tf_op jit(solution)/shard_map/slice | solution.py:377
  21.3 1.7 %collective-permute-start.4 = (bf16[32,4096]{1,0:T(8,128)(2,1)}, bf16[32,4096]{1,0:T(8,128)(2,1)}, u32[]{:S(2)}, u32[]{:S(2)}) collective-permute-start(bf16[32,4096]{1,0:T(8,128)(2,1)} %slice.13), channel_id=1, source_target_pairs={{0,2},{1,3},{2,4},{3,5},{4,6},{5,7},{6,0},{7,1},{8,10},{9,11},{10,... | collective-permute-start | bytes 786440 | tf_op jit(solution)/shard_map/ppermute | solution.py:359
  23.0 1.7 %slice.14 = bf16[32,4096]{1,0:T(8,128)(2,1)} slice(bf16[64,4096]{1,0:T(8,128)(2,1)} %collective-permute-done.1.refs_2_), slice={[32:64], [0:4096]} | slice | bytes 524288 | tf_op jit(solution)/shard_map/slice | solution.py:378
  25.0 5.6 %all-to-all-done.parts_ref = bf16[32,8,512]{2,1,0:T(8,128)(2,1)S(1)} async-done(((bf16[32,8,512]{2,1,0:T(8,128)(2,1)}), bf16[32,8,512]{2,1,0:T(8,128)(2,1)S(1)}, u32[]{:S(2)}, u32[]{:S(2)}) %all-to-all-start) | async-done | bytes 262176 | tf_op jit(solution)/shard_map/all_to_all | solution.py:374
  31.3 5.0 %all-to-all-start.1 = ((f32[8,8,512]{2,1,0:T(8,128)}), f32[8,8,512]{2,1,0:T(8,128)S(1)}, u32[]{:S(2)}, u32[]{:S(2)}) async-start(f32[8,8,512]{2,1,0:T(8,128)} %modulation_sum.1), calls=%async_computation.1 | async-start | bytes 262144 | tf_op jit(solution)/shard_map/all_to_all | solution.py:382
  38.3 2.0 %all-to-all-done.1.refs_10_.mod_ref = f32[8,8,512]{2,1,0:T(8,128)S(1)} async-done(((f32[8,8,512]{2,1,0:T(8,128)}), f32[8,8,512]{2,1,0:T(8,128)S(1)}, u32[]{:S(2)}, u32[]{:S(2)}) %all-to-all-start.1) | async-done | bytes 131104 | tf_op jit(solution)/shard_map/all_to_all | solution.py:382
  40.3 1.2 %copy-done.8 = bf16[4096,128]{1,0:T(8,128)(2,1)S(1)} copy-done((bf16[4096,128]{1,0:T(8,128)(2,1)S(1)}, bf16[4096,128]{1,0:T(8,128)(2,1)}, u32[]{:S(2)}) %copy-start.8) | copy-done | bytes 1048600
  41.5 1.2 %copy-done.9 = bf16[4096,128]{1,0:T(8,128)(2,1)S(1)} copy-done((bf16[4096,128]{1,0:T(8,128)(2,1)S(1)}, bf16[4096,128]{1,0:T(8,128)(2,1)}, u32[]{:S(2)}) %copy-start.9) | copy-done | bytes 1048600
  42.8 1.5 %context_pairs.1 = bf16[32,32,256]{2,1,0:T(8,128)(2,1)} custom-call(bf16[32,4096]{1,0:T(8,128)(2,1)S(1)} %copy-done.12, f32[8,8,512]{2,1,0:T(8,128)S(1)} %all-to-all-done.1.refs_10_.mod_ref, bf16[4096,128]{1,0:T(8,128)(2,1)S(1)} %copy-done.8, bf16[4096,128]{1,0:T(8,128)(2,1)S(1)} %copy-done.9), custom_call_target="tpu_custom_call" | custom-call | flops 2000000000 | bytes 3000000 | tf_op jit(solution)/shard_map/context_pairs/pallas_call | solution.py:110
  44.3 5.4 %all-to-all-start.2 = ((bf16[32,32,256]{2,1,0:T(8,128)(2,1)}), bf16[32,32,256]{2,1,0:T(8,128)(2,1)S(1)}, u32[]{:S(2)}, u32[]{:S(2)}) async-start(bf16[32,32,256]{2,1,0:T(8,128)(2,1)} %context_pairs.1), calls=%async_computation.2 | async-start | bytes 1048576 | tf_op jit(solution)/shard_map/all_to_all | solution.py:387
  49.7 1.0 sine_multiply_fusion
  50.8 1.0 copy-done.11
  51.8 12.3 %projections.1 = (bf16[512,256]{1,0:T(8,128)(2,1)S(1)}, bf16[512,256]{1,0:T(8,128)(2,1)S(1)}, bf16[128,256]{1,0:T(8,128)(2,1)S(1)}, bf16[128,256]{1,0:T(8,128)(2,1)S(1)}) custom-call(s32[4]{0:T(128)S(1)} %pad_add_fusion.index_ref.place_ref, bf16[64,4096]{1,0:T(8,128)(2,1)S(1)} %copy-done.2, bf16[64,4096]{1,0:T(8,128)(2,1)S(1)} %copy-done.11, ...), custom_call_target="tpu_custom_call" | custom-call | flops 8000000000 | bytes 8000000 | tf_op jit(solution)/shard_map/projections/pallas_call | solution.py:214
  65.6 4.6 %collective-permute-start.10 = (bf16[128,256]{1,0:T(8,128)(2,1)S(1)}, bf16[128,256]{1,0:T(8,128)(2,1)S(1)}, u32[]{:S(2)}, u32[]{:S(2)}) collective-permute-start(bf16[128,256]{1,0:T(8,128)(2,1)S(1)} %get-tuple-element.23), channel_id=1, source_target_pairs={{8,0},{16,8},{24,16},{32,24},{40,32},{48,40},{56,48},{64,56},{72,6... | collective-permute-start | bytes 196616 | tf_op jit(solution)/shard_map/ppermute | solution.py:403
  70.1 1.9 %collective-permute-start.9 = (bf16[128,256]{1,0:T(8,128)(2,1)S(1)}, bf16[128,256]{1,0:T(8,128)(2,1)S(1)}, u32[]{:S(2)}, u32[]{:S(2)}) collective-permute-start(bf16[128,256]{1,0:T(8,128)(2,1)S(1)} %get-tuple-element.22), channel_id=1, source_target_pairs={{0,8},{8,16},{16,24},{24,32},{32,40},{40,48},{48,56},{56,64},{64,7... | collective-permute-start | bytes 196616 | tf_op jit(solution)/shard_map/ppermute | solution.py:402
  72.1 6.3 %collective-permute-done.9.before_ref = bf16[128,256]{1,0:T(8,128)(2,1)S(1)} collective-permute-done((bf16[128,256]{1,0:T(8,128)(2,1)S(1)}, bf16[128,256]{1,0:T(8,128)(2,1)S(1)}, u32[]{:S(2)}, u32[]{:S(2)}) %collective-permute-start.9) | collective-permute-done | bytes 65568 | tf_op jit(solution)/shard_map/ppermute | solution.py:402
  78.4 0.9 copy-done.15
  79.4 0.9 copy-done.17
  80.3 1.7 %attention_1.1 = (bf16[64,256]{1,0:T(8,128)(2,1)S(1)}, bf16[64,256]{1,0:T(8,128)(2,1)S(1)}) custom-call(s32[4]{0:T(128)S(1)} %pad_add_fusion.index_ref.place_ref, f32[16]{0:T(128)S(1)} %copy-done.13, bf16[512,256]{1,0:T(8,128)(2,1)S(1)} %copy-done.15, bf16[512,256]{1,0:T(8,128)(2,1)S(1)} %copy-done.17, ...), custom_call_target="tpu_custom_call" | custom-call | flops 1500000000 | bytes 2000000 | tf_op jit(solution)/shard_map/attention_1/pallas_call | solution.py:296
  82.1 2.9 %attention_3.1 = (bf16[192,256]{1,0:T(8,128)(2,1)S(1)}, bf16[192,256]{1,0:T(8,128)(2,1)S(1)}) custom-call(s32[4]{0:T(128)S(1)} %pad_add_fusion.index_ref.place_ref, f32[16]{0:T(128)S(1)} %copy-done.13, bf16[512,256]{1,0:T(8,128)(2,1)S(1)} %copy-done.15, bf16[512,256]{1,0:T(8,128)(2,1)S(1)} %copy-done.17, ...), custom_call_target="tpu_custom_call" | custom-call | flops 4499999744 | bytes 2000000 | tf_op jit(solution)/shard_map/attention_3/pallas_call | solution.py:296
  85.6 2.1 %out_projection_64.1 = (bf16[32,4096]{1,0:T(8,128)(2,1)S(1)}, bf16[32,4096]{1,0:T(8,128)(2,1)S(1)}) custom-call(bf16[64,256]{1,0:T(8,128)(2,1)S(1)} %get-tuple-element.28.mine_ref, bf16[64,256]{1,0:T(8,128)(2,1)S(1)} %collective-permute-done.13.other_ref, bf16[256,4096]{1,0:T(8,128)(2,1)S(1)} %copy-done, ...), custom_call_target="tpu_custom_call" | custom-call | flops 1073741824 | bytes 4000000 | tf_op jit(solution)/shard_map/out_projection_64/pallas_call | solution.py:320
  87.8 2.2 %collective-permute-start.14 = (bf16[32,4096]{1,0:T(8,128)(2,1)S(1)}, bf16[32,4096]{1,0:T(8,128)(2,1)S(1)}, u32[]{:S(2)}, u32[]{:S(2)}) collective-permute-start(bf16[32,4096]{1,0:T(8,128)(2,1)S(1)} %get-tuple-element.30), channel_id=1, source_target_pairs={{0,2},{1,3},{2,4},{3,5},{4,6},{5,7},{6,0},{7,1},{8,10},{9,11},{10,... | collective-permute-start | bytes 786440 | tf_op jit(solution)/shard_map/ppermute | solution.py:359
  89.9 5.5 %out_projection_192.1 = (bf16[32,4096]{1,0:T(8,128)(2,1)S(1)}, bf16[32,4096]{1,0:T(8,128)(2,1)S(1)}, bf16[32,4096]{1,0:T(8,128)(2,1)S(1)}, bf16[32,4096]{1,0:T(8,128)(2,1)S(1)}, f32[64,4096]{1,0:T(8,128)S(1)}) custom-call(bf16[192,256]{1,0:T(8,128)(2,1)S(1)} %get-tuple-element.24.mine_ref, bf16[192,256]{1,0:T(8,128)(2,1)S(1)} %collective-permute-done.11.other_ref, ...), custom_call_target="tpu_custom_call" | custom-call | flops 3221225472 | bytes 4000000 | tf_op jit(solution)/shard_map/out_projection_192/pallas_call | solution.py:320
  95.9 3.1 %collective-permute-start.17 = (bf16[32,4096]{1,0:T(8,128)(2,1)S(1)}, bf16[32,4096]{1,0:T(8,128)(2,1)S(1)}, u32[]{:S(2)}, u32[]{:S(2)}) collective-permute-start(bf16[32,4096]{1,0:T(8,128)(2,1)S(1)} %get-tuple-element.32), channel_id=1, source_target_pairs={{0,2},{1,3},{2,4},{3,5},{4,6},{5,7},{6,0},{7,1},{8,10},{9,11},{10,... | collective-permute-start | bytes 786440 | tf_op jit(solution)/shard_map/ppermute | solution.py:359
  99.1 2.0 %collective-permute-start.15 = (bf16[32,4096]{1,0:T(8,128)(2,1)S(1)}, bf16[32,4096]{1,0:T(8,128)(2,1)S(1)}, u32[]{:S(2)}, u32[]{:S(2)}) collective-permute-start(bf16[32,4096]{1,0:T(8,128)(2,1)S(1)} %add_convert_fusion.1), channel_id=1, source_target_pairs={{0,2},{1,3},{2,4},{3,5},{4,6},{5,7},{6,0},{7,1},{8,10},{9,11},{10,... | collective-permute-start | bytes 786440 | tf_op jit(solution)/shard_map/ppermute | solution.py:359
  101.1 9.4 %collective-permute-done.18 = bf16[32,4096]{1,0:T(8,128)(2,1)S(1)} collective-permute-done((bf16[32,4096]{1,0:T(8,128)(2,1)S(1)}, bf16[32,4096]{1,0:T(8,128)(2,1)S(1)}, u32[]{:S(2)}, u32[]{:S(2)}) %collective-permute-start.18) | collective-permute-done | bytes 262176 | tf_op jit(solution)/shard_map/ppermute | solution.py:362
  110.8 8.2 %collective-permute-done.19 = bf16[32,4096]{1,0:T(8,128)(2,1)S(1)} collective-permute-done((bf16[32,4096]{1,0:T(8,128)(2,1)S(1)}, bf16[32,4096]{1,0:T(8,128)(2,1)S(1)}, u32[]{:S(2)}, u32[]{:S(2)}) %collective-permute-start.19) | collective-permute-done | bytes 262176 | tf_op jit(solution)/shard_map/ppermute | solution.py:362
  119.0 1.0 fusion.2
  (71 shorter events, 10.4 us)
Async XLA Ops:
  0.0 19.7 %collective-permute-start.3 = (bf16[64,4096]{1,0:T(8,128)(2,1)}, bf16[64,4096]{1,0:T(8,128)(2,1)}, u32[]{:S(2)}, u32[]{:S(2)}) collective-permute-start(bf16[64,4096]{1,0:T(8,128)(2,1)} %refs_0_.1), channel_id=1, source_target_pairs={{0,2},{1,3},{2,4},{3,5},{4,6},{5,7},{6,0},{7,1},{8,10},{9,11},{10,... | collective-permute-start | bytes 1572872 | tf_op jit(solution)/shard_map/ppermute | solution.py:359
  0.5 22.5 %collective-permute-start.1 = (bf16[64,4096]{1,0:T(8,128)(2,1)}, bf16[64,4096]{1,0:T(8,128)(2,1)}, u32[]{:S(2)}, u32[]{:S(2)}) collective-permute-start(bf16[64,4096]{1,0:T(8,128)(2,1)} %refs_0_.1), channel_id=1, source_target_pairs={{0,6},{1,7},{2,0},{3,1},{4,2},{5,3},{6,4},{7,5},{8,14},{9,15},{10,... | collective-permute-start | bytes 1572872 | tf_op jit(solution)/shard_map/ppermute | solution.py:362
  6.3 34.1 %copy-start.12 = (bf16[32,4096]{1,0:T(8,128)(2,1)S(1)}, bf16[32,4096]{1,0:T(8,128)(2,1)}, u32[]{:S(2)}) copy-start(bf16[32,4096]{1,0:T(8,128)(2,1)} %ctx_ref.1) | copy-start | bytes 786436
  7.7 22.9 %all-to-all-start = ((bf16[32,8,512]{2,1,0:T(8,128)(2,1)}), bf16[32,8,512]{2,1,0:T(8,128)(2,1)S(1)}, u32[]{:S(2)}, u32[]{:S(2)}) async-start(bf16[32,8,512]{2,1,0:T(8,128)(2,1)} %modulation_part.1), calls=%async_computation | async-start | bytes 524288 | tf_op jit(solution)/shard_map/all_to_all | solution.py:374
  19.1 17.5 %collective-permute-start = (bf16[64,4096]{1,0:T(8,128)(2,1)}, bf16[64,4096]{1,0:T(8,128)(2,1)S(1)}, u32[]{:S(2)}, u32[]{:S(2)}) collective-permute-start(bf16[64,4096]{1,0:T(8,128)(2,1)} %refs_0_.1), channel_id=1, source_target_pairs={{0,1},{1,0},{2,3},{3,2},{4,5},{5,4},{6,7},{7,6},{8,9},{9,8},{10,11... | collective-permute-start | bytes 1572872 | tf_op jit(solution)/shard_map/ppermute | solution.py:365
  19.2 66.5 %collective-permute-start.12 = (bf16[256,4096]{1,0:T(8,128)(2,1)}, bf16[256,4096]{1,0:T(8,128)(2,1)S(1)}, u32[]{:S(2)}, u32[]{:S(2)}) collective-permute-start(bf16[256,4096]{1,0:T(8,128)(2,1)} %w_mine_ref.3), channel_id=1, source_target_pairs={{0,1},{1,0},{2,3},{3,2},{4,5},{5,4},{6,7},{7,6},{8,9},{9,8},{10,11... | collective-permute-start | bytes 6291464 | tf_op jit(solution)/shard_map/ppermute | solution.py:365
  21.3 16.4 %collective-permute-start.4 = (bf16[32,4096]{1,0:T(8,128)(2,1)}, bf16[32,4096]{1,0:T(8,128)(2,1)}, u32[]{:S(2)}, u32[]{:S(2)}) collective-permute-start(bf16[32,4096]{1,0:T(8,128)(2,1)} %slice.13), channel_id=1, source_target_pairs={{0,2},{1,3},{2,4},{3,5},{4,6},{5,7},{6,0},{7,1},{8,10},{9,11},{10,... | collective-permute-start | bytes 786440 | tf_op jit(solution)/shard_map/ppermute | solution.py:359
  24.7 13.2 %collective-permute-start.5 = (bf16[32,4096]{1,0:T(8,128)(2,1)}, bf16[32,4096]{1,0:T(8,128)(2,1)}, u32[]{:S(2)}, u32[]{:S(2)}) collective-permute-start(bf16[32,4096]{1,0:T(8,128)(2,1)} %slice.14), channel_id=1, source_target_pairs={{0,6},{1,7},{2,0},{3,1},{4,2},{5,3},{6,4},{7,5},{8,14},{9,15},{10,... | collective-permute-start | bytes 786440 | tf_op jit(solution)/shard_map/ppermute | solution.py:362
  31.3 9.0 %all-to-all-start.1 = ((f32[8,8,512]{2,1,0:T(8,128)}), f32[8,8,512]{2,1,0:T(8,128)S(1)}, u32[]{:S(2)}, u32[]{:S(2)}) async-start(f32[8,8,512]{2,1,0:T(8,128)} %modulation_sum.1), calls=%async_computation.1 | async-start | bytes 262144 | tf_op jit(solution)/shard_map/all_to_all | solution.py:382
  36.3 14.5 %collective-permute-start.2 = (bf16[64,4096]{1,0:T(8,128)(2,1)}, bf16[64,4096]{1,0:T(8,128)(2,1)}, u32[]{:S(2)}, u32[]{:S(2)}) collective-permute-start(bf16[64,4096]{1,0:T(8,128)(2,1)} %collective-permute-done.1.refs_2_), channel_id=1, source_target_pairs={{0,1},{1,0},{2,3},{3,2},{4,5},{5,4},{6,7},{7,6},{8,9},{9,8},{10,11... | collective-permute-start | bytes 1572872 | tf_op jit(solution)/shard_map/ppermute | solution.py:365
  37.3 13.5 %collective-permute-start.8 = (bf16[64,4096]{1,0:T(8,128)(2,1)}, bf16[64,4096]{1,0:T(8,128)(2,1)}, u32[]{:S(2)}, u32[]{:S(2)}) collective-permute-start(bf16[64,4096]{1,0:T(8,128)(2,1)} %collective-permute-done.3.refs_8_), channel_id=1, source_target_pairs={{0,1},{1,0},{2,3},{3,2},{4,5},{5,4},{6,7},{7,6},{8,9},{9,8},{10,11... | collective-permute-start | bytes 1572872 | tf_op jit(solution)/shard_map/ppermute | solution.py:365
  37.7 13.1 %copy-start.2 = (bf16[64,4096]{1,0:T(8,128)(2,1)S(1)}, bf16[64,4096]{1,0:T(8,128)(2,1)}, u32[]{:S(2)}) copy-start(bf16[64,4096]{1,0:T(8,128)(2,1)} %refs_0_.1) | copy-start | bytes 1572868
  37.7 13.0 %collective-permute-start.6 = (bf16[32,4096]{1,0:T(8,128)(2,1)}, bf16[32,4096]{1,0:T(8,128)(2,1)}, u32[]{:S(2)}, u32[]{:S(2)}) collective-permute-start(bf16[32,4096]{1,0:T(8,128)(2,1)} %collective-permute-done.4.refs_4_), channel_id=1, source_target_pairs={{0,1},{1,0},{2,3},{3,2},{4,5},{5,4},{6,7},{7,6},{8,9},{9,8},{10,11... | collective-permute-start | bytes 786440 | tf_op jit(solution)/shard_map/ppermute | solution.py:365
  37.9 12.8 %collective-permute-start.7 = (bf16[32,4096]{1,0:T(8,128)(2,1)}, bf16[32,4096]{1,0:T(8,128)(2,1)}, u32[]{:S(2)}, u32[]{:S(2)}) collective-permute-start(bf16[32,4096]{1,0:T(8,128)(2,1)} %collective-permute-done.5.refs_5_), channel_id=1, source_target_pairs={{0,1},{1,0},{2,3},{3,2},{4,5},{5,4},{6,7},{7,6},{8,9},{9,8},{10,11... | collective-permute-start | bytes 786440 | tf_op jit(solution)/shard_map/ppermute | solution.py:365
  40.3 1.2 %copy-start.8 = (bf16[4096,128]{1,0:T(8,128)(2,1)S(1)}, bf16[4096,128]{1,0:T(8,128)(2,1)}, u32[]{:S(2)}) copy-start(bf16[4096,128]{1,0:T(8,128)(2,1)} %key_ref.1) | copy-start | bytes 3145732
  41.5 1.2 %copy-start.9 = (bf16[4096,128]{1,0:T(8,128)(2,1)S(1)}, bf16[4096,128]{1,0:T(8,128)(2,1)}, u32[]{:S(2)}) copy-start(bf16[4096,128]{1,0:T(8,128)(2,1)} %value_ref.1) | copy-start | bytes 3145732
  44.3 34.1 %all-to-all-start.2 = ((bf16[32,32,256]{2,1,0:T(8,128)(2,1)}), bf16[32,32,256]{2,1,0:T(8,128)(2,1)S(1)}, u32[]{:S(2)}, u32[]{:S(2)}) async-start(bf16[32,32,256]{2,1,0:T(8,128)(2,1)} %context_pairs.1), calls=%async_computation.2 | async-start | bytes 1048576 | tf_op jit(solution)/shard_map/all_to_all | solution.py:387
  50.8 1.0 copy-start.11
  51.8 26.6 %copy-start.13 = (f32[16]{0:T(128)S(1)}, f32[16]{0:T(128)}, u32[]{:S(2)}) copy-start(f32[16]{0:T(128)} %sink_ref.3) | copy-start | bytes 196
  65.6 6.5 %collective-permute-start.10 = (bf16[128,256]{1,0:T(8,128)(2,1)S(1)}, bf16[128,256]{1,0:T(8,128)(2,1)S(1)}, u32[]{:S(2)}, u32[]{:S(2)}) collective-permute-start(bf16[128,256]{1,0:T(8,128)(2,1)S(1)} %get-tuple-element.23), channel_id=1, source_target_pairs={{8,0},{16,8},{24,16},{32,24},{40,32},{48,40},{56,48},{64,56},{72,6... | collective-permute-start | bytes 196616 | tf_op jit(solution)/shard_map/ppermute | solution.py:403
  70.1 8.3 %collective-permute-start.9 = (bf16[128,256]{1,0:T(8,128)(2,1)S(1)}, bf16[128,256]{1,0:T(8,128)(2,1)S(1)}, u32[]{:S(2)}, u32[]{:S(2)}) collective-permute-start(bf16[128,256]{1,0:T(8,128)(2,1)S(1)} %get-tuple-element.22), channel_id=1, source_target_pairs={{0,8},{8,16},{16,24},{24,32},{32,40},{40,48},{48,56},{56,64},{64,7... | collective-permute-start | bytes 196616 | tf_op jit(solution)/shard_map/ppermute | solution.py:402
  78.4 1.0 copy-start.15
  82.0 3.6 %copy-start = (bf16[256,4096]{1,0:T(8,128)(2,1)S(1)}, bf16[256,4096]{1,0:T(8,128)(2,1)}, u32[]{:S(2)}) copy-start(bf16[256,4096]{1,0:T(8,128)(2,1)} %w_mine_ref.3) | copy-start | bytes 6291460
  82.0 3.6 %collective-permute-start.13 = (bf16[64,256]{1,0:T(8,128)(2,1)S(1)}, bf16[64,256]{1,0:T(8,128)(2,1)S(1)}, u32[]{:S(2)}, u32[]{:S(2)}) collective-permute-start(bf16[64,256]{1,0:T(8,128)(2,1)S(1)} %get-tuple-element.29), channel_id=1, source_target_pairs={{0,1},{1,0},{2,3},{3,2},{4,5},{5,4},{6,7},{7,6},{8,9},{9,8},{10,11... | collective-permute-start | bytes 98312 | tf_op jit(solution)/shard_map/ppermute | solution.py:365
  85.0 4.9 %collective-permute-start.11 = (bf16[192,256]{1,0:T(8,128)(2,1)S(1)}, bf16[192,256]{1,0:T(8,128)(2,1)S(1)}, u32[]{:S(2)}, u32[]{:S(2)}) collective-permute-start(bf16[192,256]{1,0:T(8,128)(2,1)S(1)} %get-tuple-element.25), channel_id=1, source_target_pairs={{0,1},{1,0},{2,3},{3,2},{4,5},{5,4},{6,7},{7,6},{8,9},{9,8},{10,11... | collective-permute-start | bytes 294920 | tf_op jit(solution)/shard_map/ppermute | solution.py:365
  85.6 2.2 %copy-start.1 = (bf16[256,4096]{1,0:T(8,128)(2,1)}, bf16[256,4096]{1,0:T(8,128)(2,1)S(1)}, u32[]{:S(2)}) copy-start(bf16[256,4096]{1,0:T(8,128)(2,1)S(1)} %collective-permute-done.12.w_other_ref) | copy-start | bytes 6291460
  87.8 11.2 %collective-permute-start.14 = (bf16[32,4096]{1,0:T(8,128)(2,1)S(1)}, bf16[32,4096]{1,0:T(8,128)(2,1)S(1)}, u32[]{:S(2)}, u32[]{:S(2)}) collective-permute-start(bf16[32,4096]{1,0:T(8,128)(2,1)S(1)} %get-tuple-element.30), channel_id=1, source_target_pairs={{0,2},{1,3},{2,4},{3,5},{4,6},{5,7},{6,0},{7,1},{8,10},{9,11},{10,... | collective-permute-start | bytes 786440 | tf_op jit(solution)/shard_map/ppermute | solution.py:359
  95.4 15.3 %collective-permute-start.16 = (bf16[32,4096]{1,0:T(8,128)(2,1)S(1)}, bf16[32,4096]{1,0:T(8,128)(2,1)S(1)}, u32[]{:S(2)}, u32[]{:S(2)}) collective-permute-start(bf16[32,4096]{1,0:T(8,128)(2,1)S(1)} %get-tuple-element.31), channel_id=1, source_target_pairs={{0,6},{1,7},{2,0},{3,1},{4,2},{5,3},{6,4},{7,5},{8,14},{9,15},{10,... | collective-permute-start | bytes 786440 | tf_op jit(solution)/shard_map/ppermute | solution.py:362
  95.7 14.8 %collective-permute-start.18 = (bf16[32,4096]{1,0:T(8,128)(2,1)S(1)}, bf16[32,4096]{1,0:T(8,128)(2,1)S(1)}, u32[]{:S(2)}, u32[]{:S(2)}) collective-permute-start(bf16[32,4096]{1,0:T(8,128)(2,1)S(1)} %get-tuple-element.34), channel_id=1, source_target_pairs={{0,6},{1,7},{2,0},{3,1},{4,2},{5,3},{6,4},{7,5},{8,14},{9,15},{10,... | collective-permute-start | bytes 786440 | tf_op jit(solution)/shard_map/ppermute | solution.py:362
  95.9 14.8 %collective-permute-start.17 = (bf16[32,4096]{1,0:T(8,128)(2,1)S(1)}, bf16[32,4096]{1,0:T(8,128)(2,1)S(1)}, u32[]{:S(2)}, u32[]{:S(2)}) collective-permute-start(bf16[32,4096]{1,0:T(8,128)(2,1)S(1)} %get-tuple-element.32), channel_id=1, source_target_pairs={{0,2},{1,3},{2,4},{3,5},{4,6},{5,7},{6,0},{7,1},{8,10},{9,11},{10,... | collective-permute-start | bytes 786440 | tf_op jit(solution)/shard_map/ppermute | solution.py:359
  99.1 11.6 %collective-permute-start.15 = (bf16[32,4096]{1,0:T(8,128)(2,1)S(1)}, bf16[32,4096]{1,0:T(8,128)(2,1)S(1)}, u32[]{:S(2)}, u32[]{:S(2)}) collective-permute-start(bf16[32,4096]{1,0:T(8,128)(2,1)S(1)} %add_convert_fusion.1), channel_id=1, source_target_pairs={{0,2},{1,3},{2,4},{3,5},{4,6},{5,7},{6,0},{7,1},{8,10},{9,11},{10,... | collective-permute-start | bytes 786440 | tf_op jit(solution)/shard_map/ppermute | solution.py:359
  110.6 8.4 %collective-permute-start.19 = (bf16[32,4096]{1,0:T(8,128)(2,1)S(1)}, bf16[32,4096]{1,0:T(8,128)(2,1)S(1)}, u32[]{:S(2)}, u32[]{:S(2)}) collective-permute-start(bf16[32,4096]{1,0:T(8,128)(2,1)S(1)} %add_convert_fusion), channel_id=1, source_target_pairs={{0,6},{1,7},{2,0},{3,1},{4,2},{5,3},{6,4},{7,5},{8,14},{9,15},{10,... | collective-permute-start | bytes 786440 | tf_op jit(solution)/shard_map/ppermute | solution.py:362
  (9 other events, 7.3 us)
